TPU v7x, 32 devices: a whole 2x2x4 slice. The times are simulated.
32 devices in a mesh: sp: 8 (over z, x), tp: 4 (over y, core).
Axes of the slice: x: 2, y: 2, z: 4, core: 2. Of those that a mesh axis runs over, the one named last changes fastest.
Arguments:
- tokens: bfloat16 [3072, 2048], P('sp'), may hold values from -6 to 6
- doc_ids: int32 [3072], P('sp'), may hold values from 0 to 2, never falling along the last dimension, each value on 1 to 2048 neighbouring positions
- pre_gain: float32 [2, 2048], replicated, may hold values from 0.1 to 1.9
- value_proj: bfloat16 [2, 2048, 1024], P(None, 'sp', 'tp'), may hold values from -0.1875 to 0.1875
- gate_proj: bfloat16 [2, 2048, 1024], P(None, 'sp', 'tp'), may hold values from -0.1875 to 0.1875
- out_proj: bfloat16 [2, 1024, 2048], P(None, 'tp', 'sp'), may hold values from -0.1875 to 0.1875
- conv_taps: float32 [2, 31, 1024], P(None, None, 'tp'), may hold values from -2.2 to 2.2
- norm_gain: float32 [2, 1024], P(None, 'tp'), may hold values from 0.1 to 1.9
- norm_shift: float32 [2, 1024], P(None, 'tp'), may hold values from -3 to 3
Outputs:
- hidden: bfloat16 [3072, 2048], P('sp')
Inputs may be any that keep to these rules, and one draw needn't show every extreme that they name: `doc_ids`: document numbers never fall along the sequence; each document has 1 to 2048 positions.
All inputs are finite; a program needn't handle non-finite values.
Results may differ from a plain program's by a relative error of at most 0.017.
Values may be sent and summed in bfloat16 or wider, within the bound.
A program may use at most 64 MiB of HBM per device.

v0:
```python
import jax
import jax.numpy as jnp
from jax import lax
from jax.sharding import PartitionSpec as P

epsilon = 1e-06


def passed_along(value, axis, steps):
    count = lax.axis_size(axis)
    first, last = (max(0, -steps), min(count, count - steps))
    return lax.ppermute(value, axis, [(source, source + steps) for source in range(first, last)])


def on_device(
    tokens, doc_ids, pre_gain, value_proj, gate_proj, out_proj, conv_taps, norm_gain, norm_shift
):
    layer_count = value_proj.shape[0]
    tap_count = conv_taps.shape[1]
    reach_rows = tap_count - 1
    row_count = tokens.shape[0]
    block_width = conv_taps.shape[2]
    channels = block_width * lax.axis_size("tp")
    hidden = tokens
    full_value, full_gate, full_out = (
        lax.all_gather(value_proj, "sp", axis=1, tiled=True),
        lax.all_gather(gate_proj, "sp", axis=1, tiled=True),
        lax.all_gather(out_proj, "sp", axis=2, tiled=True),
    )
    for layer_index in range(layer_count):
        wide_state = hidden.astype(jnp.float32)
        scale = lax.rsqrt(jnp.mean(wide_state * wide_state, axis=-1, keepdims=True) + epsilon)
        normed = (wide_state * scale * pre_gain[layer_index]).astype(jnp.bfloat16)
        value_acc = jnp.dot(normed, full_value[layer_index], preferred_element_type=jnp.float32)
        gate_acc = jnp.dot(normed, full_gate[layer_index], preferred_element_type=jnp.float32)
        value_half = value_acc.astype(jnp.bfloat16)
        gate_half = gate_acc.astype(jnp.bfloat16)
        gated_rows = (
            value_half.astype(jnp.float32) * jax.nn.sigmoid(gate_half.astype(jnp.float32))
        ).astype(jnp.bfloat16)
        prev_rows, prev_docs = passed_along(
            (gated_rows[row_count - reach_rows :], doc_ids[row_count - reach_rows :]), "sp", 1
        )
        padded = jnp.concatenate([prev_rows, gated_rows]).astype(jnp.float32)
        padded_docs = jnp.concatenate([prev_docs, doc_ids])
        conv_out = jnp.zeros((row_count, block_width), jnp.float32)
        for offset in range(tap_count):
            first_row = reach_rows - offset
            same_doc = (padded_docs[first_row : first_row + row_count] == doc_ids)[:, None]
            term = (
                conv_taps[layer_index, offset][None, :] * padded[first_row : first_row + row_count]
            )
            conv_out = conv_out + jnp.where(same_doc, term, jnp.float32(0.0))
        row_sums, square_sums = lax.psum(
            (jnp.sum(conv_out, axis=1), jnp.sum(conv_out * conv_out, axis=1)), "tp"
        )
        row_mean = (row_sums / channels)[:, None]
        row_var = (square_sums / channels)[:, None] - row_mean * row_mean
        normalized = (
            norm_gain[layer_index] * (conv_out - row_mean) * lax.rsqrt(row_var + epsilon)
            + norm_shift[layer_index]
        )
        activated = jax.nn.silu(normalized).astype(jnp.bfloat16)
        partial_value = jnp.dot(
            activated, full_out[layer_index], preferred_element_type=jnp.float32
        )
        summed = lax.psum(partial_value.astype(jnp.bfloat16), "tp")
        hidden = (hidden.astype(jnp.float32) + summed.astype(jnp.float32)).astype(jnp.bfloat16)
    return hidden


def solution(mesh):
    return jax.shard_map(
        on_device,
        mesh=mesh,
        in_specs=(
            P("sp", None),
            P("sp"),
            P(),
            P(None, "sp", "tp"),
            P(None, "sp", "tp"),
            P(None, "tp", "sp"),
            P(None, None, "tp"),
            P(None, "tp"),
            P(None, "tp"),
        ),
        out_specs=P("sp", None),
        check_vma=False,
    )
```

profile of v0, /device:TPU:0, one launch (start us, length us, event | category | flops | bytes accessed | tf_op | source)
XLA Modules:
  0.0 281.7 jit_solution(4134798259272036803)
XLA Ops:
  6.5 0.0 copy-start.5
  6.6 0.0 all-gather.4.cloned.1.call-start
  6.6 0.7 all-gather.4.cloned.1.call-update
  7.3 0.0 all-gather.6.cloned.1.call-start
  7.3 0.7 all-gather.6.cloned.1.call-update
  8.0 0.0 all-gather.8.cloned.1.call-start
  8.1 0.8 slice.545
  8.8 4.9 %collective-permute-start.1 = (s32[30]{0:T(128)S(1)}, s32[30]{0:T(128)S(1)}, u32[]{:S(2)}, u32[]{:S(2)}) collective-permute-start(s32[30]{0:T(128)S(1)} %slice.545), channel_id=1, source_target_pairs={{0,4},{4,8},{8,12},{12,16},{16,20},{20,24},{24,28},{1,5},{5,9},{9,... | collective-permute-start | bytes 368 | tf_op jit(solution)/shard_map/ppermute | solution.py:12
  13.7 0.0 all-gather.8.cloned.1.call-update
  13.7 0.0 all-reduce.5.cloned.1.call-start
  13.8 1.8 fusion
  15.6 0.0 copy-done.1
  15.6 0.0 copy-done.4
  15.7 0.0 copy-done.3
  15.7 0.0 copy-done.5
  15.7 0.0 collective-permute-done.1
  15.8 0.0 copy-done.2
  15.8 0.1 pad_add_fusion
  15.8 0.1 slice_compare_fusion.29
  15.9 45.4 %all-gather.4.cloned.1.call-done = bf16[2,2048,256]{2,1,0:T(8,128)(2,1)} async-done(((bf16[2,256,256]{2,1,0:T(8,128)(2,1)}), bf16[2,2048,256]{2,1,0:T(8,128)(2,1)}) %all-gather.4.cloned.1.call-update) | async-done | bytes 2097168 | tf_op jit(solution)/shard_map/all_gather | solution.py:26
  61.4 0.0 copy-done
  61.4 1.8 fusion.23
  63.2 48.0 %all-gather.6.cloned.1.call-done = bf16[2,2048,256]{2,1,0:T(8,128)(2,1)} async-done(((bf16[2,256,256]{2,1,0:T(8,128)(2,1)}), bf16[2,2048,256]{2,1,0:T(8,128)(2,1)}) %all-gather.6.cloned.1.call-update) | async-done | bytes 2097168 | tf_op jit(solution)/shard_map/all_gather | solution.py:27
  111.2 1.9 fusion.22
  113.1 2.5 collective-permute-start
  115.5 0.1 slice_compare_fusion.28
  115.6 1.3 collective-permute-done
  117.0 3.3 %fusion.161 = (f32[384]{0:T(512)S(1)}, f32[384]{0:T(512)S(1)}, f32[384,256]{1,0:T(8,128)S(1)}) fusion(f32[414,256]{1,0:T(8,128)S(1)} %maximum_convert_fusion, f32[256]{0:T(256)S(1)} %bitcast.124, pred[384]{0:T(512)(128)(4,1)S(1)} %get-tuple-element.109, f32[256]{0:T(256)S(1)} %bitcast.125, pred[384]{0:T(512)(128)(4,1)S(1)} %get-tuple-element.110, ...), kind=kLoop, calls=%fused_computation.280 | loop fusion | flops 9239808 | bytes 12629248 | tf_op jit(solution)/shard_map/reduce_sum | solution.py:55
  120.4 6.1 %all-reduce.1 = (f32[384]{0:T(512)S(1)}, f32[384]{0:T(512)S(1)}) all-reduce(f32[384]{0:T(512)S(1)} %get-tuple-element.8, f32[384]{0:T(512)S(1)} %get-tuple-element.7), channel_id=1, replica_groups=mesh['sp'=8,'tp'=4] {'tp'}, use_global_device_ids=true, to_apply=%region_4.5 | all-reduce | flops 768 | bytes 6144 | tf_op jit(solution)/shard_map/psum | solution.py:54
  126.4 35.7 %all-gather.8.cloned.1.call-done = bf16[2,256,2048]{2,1,0:T(8,128)(2,1)} async-done(((bf16[2,256,256]{2,1,0:T(8,128)(2,1)}), bf16[2,256,2048]{2,1,0:T(8,128)(2,1)}) %all-gather.8.cloned.1.call-update) | async-done | bytes 2097168 | tf_op jit(solution)/shard_map/all_gather | solution.py:28
  162.1 3.0 %convolution_convert_fusion.1 = bf16[384,2048]{1,0:T(8,128)(2,1)} fusion(bf16[2,256,2048]{2,1,0:T(8,128)(2,1)} %all-gather.8.cloned.1.call-done, f32[384,256]{1,0:T(8,128)S(1)} %get-tuple-element.16, f32[256]{0:T(256)S(1)} %bitcast.155, f32[384]{0:T(512)S(1)} %get-tuple-element.118, f32[384]{0:T(512)S(1)} %get-tuple-element.117, f32[256]{0:T(256)S(1)} %bitcast.154), kind=kOutput, calls=%fused_computation.15 | convolution fusion | flops 404324352 | bytes 3019776 | tf_op jit(solution)/shard_map/dot_general | solution.py:64
  165.1 0.0 all-reduce.5.cloned.1.call-update
  165.2 0.0 all-reduce.7.cloned.1.call-start
  165.2 41.1 %all-reduce.5.cloned.1.call-done = bf16[384,2048]{1,0:T(8,128)(2,1)} async-done(((bf16[384,2048]{1,0:T(8,128)(2,1)}), bf16[384,2048]{1,0:T(8,128)(2,1)}) %all-reduce.5.cloned.1.call-update) | async-done | bytes 1572880 | tf_op jit(solution)/shard_map/psum | solution.py:67
  206.4 2.3 fusion.4
  208.7 0.0 copy-done.6
  208.7 0.0 copy-start.7
  208.7 0.6 fusion.15
  209.3 1.0 copy-done.7
  210.3 0.7 fusion.14
  211.0 3.4 %collective-permute-start.2 = (bf16[30,256]{1,0:T(8,128)(2,1)S(1)}, bf16[30,256]{1,0:T(8,128)(2,1)S(1)}, u32[]{:S(2)}, u32[]{:S(2)}) collective-permute-start(bf16[30,256]{1,0:T(8,128)(2,1)S(1)} %slice.744), channel_id=1, source_target_pairs={{0,4},{4,8},{8,12},{12,16},{16,20},{20,24},{24,28},{1,5},{5,9},{9,... | collective-permute-start | bytes 46088 | tf_op jit(solution)/shard_map/ppermute | solution.py:12
  214.4 1.4 collective-permute-done.2
  215.8 3.3 %fusion.160 = (f32[384]{0:T(512)S(1)}, f32[384]{0:T(512)S(1)}, f32[384,256]{1,0:T(8,128)S(1)}) fusion(f32[414,256]{1,0:T(8,128)S(1)} %maximum_convert_fusion.1, f32[256]{0:T(256)S(1)} %bitcast.90, pred[384]{0:T(512)(128)(4,1)S(1)} %get-tuple-element.109, f32[256]{0:T(256)S(1)} %bitcast.91, pred[384]{0:T(512)(128)(4,1)S(1)} %get-tuple-element.110, ...), kind=kLoop, calls=%fused_computation.279 | loop fusion | flops 9239808 | bytes 12629248 | tf_op jit(solution)/shard_map/reduce_sum | solution.py:55
  219.1 6.0 %all-reduce = (f32[384]{0:T(512)S(1)}, f32[384]{0:T(512)S(1)}) all-reduce(f32[384]{0:T(512)S(1)} %get-tuple-element.6, f32[384]{0:T(512)S(1)} %get-tuple-element.5), channel_id=1, replica_groups=mesh['sp'=8,'tp'=4] {'tp'}, use_global_device_ids=true, to_apply=%region_10.11 | all-reduce | flops 768 | bytes 6144 | tf_op jit(solution)/shard_map/psum | solution.py:54
  225.1 3.0 %convolution_convert_fusion = bf16[384,2048]{1,0:T(8,128)(2,1)} fusion(bf16[2,256,2048]{2,1,0:T(8,128)(2,1)} %all-gather.8.cloned.1.call-done, f32[384,256]{1,0:T(8,128)S(1)} %get-tuple-element.13, f32[256]{0:T(256)S(1)} %bitcast.153, f32[384]{0:T(512)S(1)} %get-tuple-element.114, f32[384]{0:T(512)S(1)} %get-tuple-element.113, f32[256]{0:T(256)S(1)} %bitcast.152), kind=kOutput, calls=%fused_computation.14 | convolution fusion | flops 404324352 | bytes 3019776 | tf_op jit(solution)/shard_map/dot_general | solution.py:64
  228.2 0.0 all-reduce.7.cloned.1.call-update
  228.2 43.8 %all-reduce.7.cloned.1.call-done = bf16[384,2048]{1,0:T(8,128)(2,1)} async-done(((bf16[384,2048]{1,0:T(8,128)(2,1)}), bf16[384,2048]{1,0:T(8,128)(2,1)}) %all-reduce.7.cloned.1.call-update) | async-done | bytes 1572880 | tf_op jit(solution)/shard_map/psum | solution.py:67
  272.0 3.2 %fusion.7 = bf16[384,2048]{1,0:T(8,128)(2,1)} fusion(bf16[384,2048]{1,0:T(8,128)(2,1)S(1)} %get-tuple-element.15, bf16[384,2048]{1,0:T(8,128)(2,1)} %all-reduce.7.cloned.1.call-done), kind=kLoop, calls=%fused_computation.13 | loop fusion | flops 3145728 | bytes 4718592 | tf_op jit(solution)/shard_map/convert_element_type | solution.py:68
  (21 shorter events, 0.2 us)
Async XLA Ops:
  6.5 9.2 %copy-start.2 = (s32[384]{0:T(512)S(1)}, s32[384]{0:T(512)}, u32[]{:S(2)}) copy-start(s32[384]{0:T(512)} %param.10) | copy-start | bytes 4612
  6.5 54.8 %copy-start = (bf16[384,2048]{1,0:T(8,128)(2,1)S(1)}, bf16[384,2048]{1,0:T(8,128)(2,1)}, u32[]{:S(2)}) copy-start(bf16[384,2048]{1,0:T(8,128)(2,1)} %param.9) | copy-start | bytes 4718596
  6.5 9.1 %copy-start.1 = (f32[2,31,256]{2,0,1:T(2,128)S(1)}, f32[2,31,256]{2,0,1:T(2,128)}, u32[]{:S(2)}) copy-start(f32[2,31,256]{2,0,1:T(2,128)} %param.15) | copy-start | bytes 190468
  6.5 9.1 %copy-start.4 = (f32[2,256]{1,0:T(2,128)S(1)}, f32[2,256]{1,0:T(2,128)}, u32[]{:S(2)}) copy-start(f32[2,256]{1,0:T(2,128)} %param.16) | copy-start | bytes 6148
  6.5 9.1 %copy-start.3 = (f32[2,2048]{1,0:T(2,128)S(1)}, f32[2,2048]{1,0:T(2,128)}, u32[]{:S(2)}) copy-start(f32[2,2048]{1,0:T(2,128)} %param.11) | copy-start | bytes 49156
  6.5 9.2 %copy-start.5 = (f32[2,256]{1,0:T(2,128)S(1)}, f32[2,256]{1,0:T(2,128)}, u32[]{:S(2)}) copy-start(f32[2,256]{1,0:T(2,128)} %param.17) | copy-start | bytes 6148
  6.6 54.8 %all-gather.4.cloned.1.call-start = ((), (), s32[]{:S(2)}) async-start(), calls=%async_computation | async-start | bytes 2359296 | tf_op jit(solution)/shard_map/all_gather | solution.py:26
  7.3 103.9 %all-gather.6.cloned.1.call-start = ((), (), s32[]{:S(2)}) async-start(), calls=%async_computation.1 | async-start | bytes 2359296 | tf_op jit(solution)/shard_map/all_gather | solution.py:27
  8.0 154.1 %all-gather.8.cloned.1.call-start = ((), (), s32[]{:S(2)}) async-start(), calls=%async_computation.2 | async-start | bytes 2359296 | tf_op jit(solution)/shard_map/all_gather | solution.py:28
  8.8 6.9 %collective-permute-start.1 = (s32[30]{0:T(128)S(1)}, s32[30]{0:T(128)S(1)}, u32[]{:S(2)}, u32[]{:S(2)}) collective-permute-start(s32[30]{0:T(128)S(1)} %slice.545), channel_id=1, source_target_pairs={{0,4},{4,8},{8,12},{12,16},{16,20},{20,24},{24,28},{1,5},{5,9},{9,... | collective-permute-start | bytes 368 | tf_op jit(solution)/shard_map/ppermute | solution.py:12
  13.7 192.6 %all-reduce.5.cloned.1.call-start = ((), (), s32[]{:S(2)}) async-start(), calls=%async_computation.3 | async-start | bytes 3145728 | tf_op jit(solution)/shard_map/psum | solution.py:67
  113.1 3.9 %collective-permute-start = (bf16[30,256]{1,0:T(8,128)(2,1)S(1)}, bf16[30,256]{1,0:T(8,128)(2,1)S(1)}, u32[]{:S(2)}, u32[]{:S(2)}) collective-permute-start(bf16[30,256]{1,0:T(8,128)(2,1)S(1)} %slice.709), channel_id=1, source_target_pairs={{0,4},{4,8},{8,12},{12,16},{16,20},{20,24},{24,28},{1,5},{5,9},{9,... | collective-permute-start | bytes 46088 | tf_op jit(solution)/shard_map/ppermute | solution.py:12
  165.2 106.9 %all-reduce.7.cloned.1.call-start = ((), (), s32[]{:S(2)}) async-start(), calls=%async_computation.4 | async-start | bytes 3145728 | tf_op jit(solution)/shard_map/psum | solution.py:67
  206.4 2.3 copy-start.6
  208.7 1.6 copy-start.7
  211.0 4.8 %collective-permute-start.2 = (bf16[30,256]{1,0:T(8,128)(2,1)S(1)}, bf16[30,256]{1,0:T(8,128)(2,1)S(1)}, u32[]{:S(2)}, u32[]{:S(2)}) collective-permute-start(bf16[30,256]{1,0:T(8,128)(2,1)S(1)} %slice.744), channel_id=1, source_target_pairs={{0,4},{4,8},{8,12},{12,16},{16,20},{20,24},{24,28},{1,5},{5,9},{9,... | collective-permute-start | bytes 46088 | tf_op jit(solution)/shard_map/ppermute | solution.py:12
Sparse Core Ops, SparseCore 0:
  9.6 51.7 all-gather.3
  63.6 47.5 all-gather.5
  113.2 48.8 all-gather.7
  165.3 41.0 all-reduce.4
  228.3 43.6 all-reduce.6
where the time goes:
time: 282 us
  waiting for transfers between devices  218 us (77%)
  other arithmetic  14.3 us (5%)
  between operations  13.4 us (5%)
  blocking collectives  12 us (4%)
  matrix products  11.1 us (4%)
  starting transfers between devices  10.9 us (4%)
    psum x2, waiting for transfers between devices, on_device(): summed = lax.psum(partial_value.astype(jnp.bfloat16), 'tp')  85 us
    all_gather x1, waiting for transfers between devices, on_device(): lax.all_gather(gate_proj, 'sp', axis=1, tiled=True)  48 us
    all_gather x1, waiting for transfers between devices, on_device(): lax.all_gather(value_proj, 'sp', axis=1, tiled=True)  45.4 us
    all_gather x1, waiting for transfers between devices, on_device(): lax.all_gather(out_proj, 'sp', axis=2, tiled=True)  35.7 us
    psum x2, blocking collectives, on_device(): lax.psum((jnp.sum(conv_out, axis=1), jnp.sum(conv_out * conv_out, axis=1)...  12 us
    ppermute x3, starting transfers between devices, passed_along(): lax.ppermute(value, axis, [(source, source + steps) for source in range(f...  10.7 us
    reduce_sum x2, other arithmetic, on_device(): jnp.sum(conv_out, axis=1)  6.66 us
    dot_general x2, matrix products, on_device(): jnp.dot(activated, full_out[layer_index], preferred_element_type=jnp.floa...  6.08 us
  transfers between devices with their start and end apart: 8, of which 7 were waited for; matrix products, arithmetic and copies ran while one was open for 4% of the time, Pallas kernels for 0%

commit v1 on v0

--- a/solution.py
+++ b/solution.py
@@ -1,9 +1,366 @@
+import functools
 import jax
 import jax.numpy as jnp
 from jax import lax
+from jax.experimental import pallas as pl
+from jax.experimental.pallas import tpu as pltpu
 from jax.sharding import PartitionSpec as P
 
 epsilon = 1e-06
+MESH = pl.DeviceIdType.MESH
+HALO = 32
+CONV_ROWS = 64
+
+
+def fused_kernel(
+    n, m, reach, layers,
+    tok_ref, doc_ref, gain_ref, v_ref, g_ref, o_ref, tap_ref, ng_ref, ns_ref,
+    out_ref,
+    w, oring, ofull, normed, acc, padded, pdoc, run, ghalo, halo_in, doc_in,
+    stat, stat_out, stat_in, conv, act_all, hid,
+    rsend, rrecv, osend, orecv, hsend, hrecv, ssend, srecv, asend, arecv, xsend, xrecv,
+):
+    me = lax.axis_index("sp")
+    t = lax.axis_index("tp")
+    q, c = t // 2, t % 2
+    pairs = m // 2
+    half_n = n // 2
+    rows, width = tok_ref.shape
+    depth, block = v_ref.shape[1], v_ref.shape[2]
+    owidth = o_ref.shape[2]
+    hd, ho = depth // 2, owidth // 2
+    half_width = width // 2
+    channels = block * m
+
+    def index_of(position):
+        position = (position + 2 * n) % n
+        return jnp.where(position < half_n, 2 * position, 2 * (n - 1 - position) + 1)
+
+    my_pos = jnp.where(me % 2 == 0, me // 2, n - 1 - me // 2)
+    right, left = index_of(my_pos + 1), index_of(my_pos - 1)
+    following, before = (me + 1) % n, (me + n - 1) % n
+
+    barrier = pltpu.get_barrier_semaphore()
+    for other in (right, left, following, before):
+        pl.semaphore_signal(barrier, inc=1, device_id={"sp": other}, device_id_type=MESH)
+    for k in range(1, m):
+        pl.semaphore_signal(barrier, inc=1, device_id={"tp": (t + k) % m}, device_id_type=MESH)
+    pl.semaphore_wait(barrier, 3 + m)
+
+    def to_sp(src, dst, send, recv, target):
+        return pltpu.make_async_remote_copy(
+            src_ref=src, dst_ref=dst, send_sem=send, recv_sem=recv,
+            device_id={"sp": target}, device_id_type=MESH)
+
+    def to_tp(src, dst, send, recv, target):
+        return pltpu.make_async_remote_copy(
+            src_ref=src, dst_ref=dst, send_sem=send, recv_sem=recv,
+            device_id={"tp": target}, device_id_type=MESH)
+
+    def w_piece(layer, owner, way, part):
+        return w.at[layer, pl.ds(pl.multiple_of(owner * depth + part * hd, hd), hd),
+                    pl.ds(way * block, block)]
+
+    def o_piece(layer, owner, way):
+        return oring.at[layer, :, pl.ds(pl.multiple_of(owner * owidth + way * ho, ho), ho)]
+
+    def ring_copy(layer, msg, way, step, own=False):
+        owner = index_of(my_pos - step if way == 0 else my_pos + step)
+        if msg < 2:
+            dst = w_piece(layer, owner, way, msg)
+            src = (v_ref, g_ref)[way].at[layer, pl.ds(msg * hd, hd), :] if own else dst
+        else:
+            dst = o_piece(layer, owner, way)
+            src = o_ref.at[layer, :, pl.ds(way * ho, ho)] if own else dst
+        return to_sp(src, dst, rsend.at[layer, msg, way, step], rrecv.at[layer, msg, way, step],
+                     right if way == 0 else left)
+
+    def arrival(layer, msg, way, step):
+        owner = index_of(my_pos - step - 1 if way == 0 else my_pos + step + 1)
+        dst = w_piece(layer, owner, way, msg) if msg < 2 else o_piece(layer, owner, way)
+        return to_sp(dst, dst, rsend.at[layer, msg, way, step], rrecv.at[layer, msg, way, step],
+                     right if way == 0 else left)
+
+    def spread_copy(layer, way, step, pair, own=False):
+        owner = index_of(my_pos - step if way == 0 else my_pos + step)
+        part = owner // half_n
+        local = owner - part * half_n
+        src = o_ref.at[layer, :, pl.ds(way * ho, ho)] if own else o_piece(layer, owner, way)
+        dst = ofull.at[layer, pl.ds(pl.multiple_of(t * block, block), block),
+                       pl.ds(pl.multiple_of(local * owidth + way * ho, ho), ho)]
+        copy = to_tp(src, dst, osend.at[layer, way, step, pair],
+                     orecv.at[layer, t, local * 2 + way], 2 * ((q + pair) % pairs) + part)
+        return copy, part
+
+    def spread(layer, way, step, act, own=False):
+        for pair in range(pairs - 1, -1, -1):
+            copy, part = spread_copy(layer, way, step, pair, own)
+            if pair == 0:
+                pl.when(part != c)(lambda copy=copy: getattr(copy, act)())
+            else:
+                getattr(copy, act)()
+
+    def open_ring(layer):
+        for msg in range(3):
+            for way in range(2):
+                ring_copy(layer, msg, way, 0, own=True).start()
+        for way in range(2):
+            spread(layer, way, 0, "start", own=True)
+
+    def keep_own(layer):
+        row = pl.ds(pl.multiple_of(me * depth, depth), depth)
+        w[layer, row, pl.ds(0, block)] = v_ref[layer]
+        w[layer, row, pl.ds(block, block)] = g_ref[layer]
+        oring[layer, :, pl.ds(pl.multiple_of(me * owidth, owidth), owidth)] = o_ref[layer]
+
+    def service(layer, first, last):
+        @pl.loop(first, last)
+        def _(step):
+            for msg in range(3):
+                for way in range(2):
+                    arrival(layer, msg, way, step - 1).wait_recv()
+                    ring_copy(layer, msg, way, step).start()
+            for way in range(2):
+                spread(layer, way, step, "start")
+
+    def finish_ring(layer):
+        for msg in range(3):
+            for way in range(2):
+                arrival(layer, msg, way, n - 2).wait_recv()
+        for way in range(2):
+            spread(layer, way, n - 1, "start")
+
+    open_ring(0)
+    doc_copy = to_sp(doc_ref.at[pl.ds(rows - HALO, HALO), :], doc_in, hsend.at[layers],
+                     hrecv.at[layers], following)
+    doc_copy.start()
+
+    def norm_rows(layer, source):
+        @pl.loop(0, rows // 32)
+        def _(i):
+            span = pl.ds(pl.multiple_of(i * 32, 32), 32)
+            wide = source[span, :].astype(jnp.float32)
+            scale = lax.rsqrt(jnp.mean(wide * wide, axis=-1, keepdims=True) + epsilon)
+            normed[span, :] = (wide * scale * gain_ref[pl.ds(layer, 1), :]).astype(jnp.bfloat16)
+
+    norm_rows(0, tok_ref)
+    keep_own(0)
+    service(0, 1, 2)
+    doc_copy.wait_recv()
+    pdoc[pl.ds(0, HALO), :] = jnp.where(me == 0, -1, doc_in[...])
+    pdoc[pl.ds(HALO, rows), :] = doc_ref[...]
+
+    @pl.loop(0, rows // CONV_ROWS)
+    def _(i):
+        base = pl.multiple_of(i * CONV_ROWS, CONV_ROWS)
+        mine = pdoc[pl.ds(base + HALO, CONV_ROWS), :]
+        count = jnp.zeros_like(mine)
+        for j in range(1, reach + 1):
+            count = count + (pdoc[pl.ds(base + (HALO - j), CONV_ROWS), :] == mine).astype(jnp.int32)
+        run[pl.ds(base, CONV_ROWS), :] = count
+
+    service(0, 2, n - 1)
+    if layers > 1:
+        for later in range(1, layers):
+            keep_own(later)
+
+    lane = lax.broadcasted_iota(jnp.int32, (CONV_ROWS, 128), 1)
+
+    def layer_step(layer, source, target):
+        nxt = layer + 1 if layer + 1 < layers else None
+        marks = iter([(1, 2), (2, 3), (3, 4), (4, 5), (5, 6), (6, n - 1)] if n == 8 else [(1, n - 1)])
+
+        def tend():
+            if nxt is not None:
+                span = next(marks, None)
+                if span is not None:
+                    service(nxt, *span)
+
+        if nxt is not None:
+            open_ring(nxt)
+        finish_ring(layer)
+        acc[...] = jnp.dot(normed[...], w[layer], preferred_element_type=jnp.float32)
+
+        def store_padded(row, values):
+            for part in range(block // 128):
+                padded[pl.ds(row + part * (rows + HALO), 32), :] = values[:, part * 128:(part + 1) * 128].astype(jnp.float32)
+
+        def gate_rows(i):
+            span = pl.ds(pl.multiple_of(i * 32, 32), 32)
+            value = acc[span, pl.ds(0, block)].astype(jnp.bfloat16).astype(jnp.float32)
+            gate = acc[span, pl.ds(block, block)].astype(jnp.bfloat16).astype(jnp.float32)
+            gated = (value * jax.nn.sigmoid(gate)).astype(jnp.bfloat16)
+            store_padded(pl.multiple_of(i * 32 + HALO, 32), gated)
+            return gated
+
+        ghalo[layer] = gate_rows(rows // 32 - 1)
+        halo_copy = to_sp(ghalo.at[layer], halo_in.at[layer], hsend.at[layer], hrecv.at[layer], following)
+        halo_copy.start()
+
+        @pl.loop(0, rows // 32 - 1)
+        def _(i):
+            gate_rows(i)
+
+        tend()
+        halo_copy.wait_recv()
+        store_padded(0, halo_in[layer])
+
+        @pl.loop(0, rows // CONV_ROWS)
+        def _(i):
+            base = pl.multiple_of(i * CONV_ROWS, CONV_ROWS)
+            count = run[pl.ds(base, CONV_ROWS), :]
+            first_sum = jnp.zeros((CONV_ROWS, 1), jnp.float32)
+            square_sum = jnp.zeros((CONV_ROWS, 1), jnp.float32)
+            for part in range(block // 128):
+                cols = pl.ds(part * 128, 128)
+                lift = part * (rows + HALO)
+                total = tap_ref[layer, pl.ds(0, 1), cols] * padded[pl.ds(base + (lift + HALO), CONV_ROWS), :]
+                for j in range(1, reach + 1):
+                    term = tap_ref[layer, pl.ds(j, 1), cols] * padded[pl.ds(base + (lift + HALO - j), CONV_ROWS), :]
+                    total = total + jnp.where(count >= j, term, jnp.float32(0.0))
+                conv[pl.ds(base, CONV_ROWS), cols] = total
+                first_sum = first_sum + jnp.sum(total, axis=1, keepdims=True)
+                square_sum = square_sum + jnp.sum(total * total, axis=1, keepdims=True)
+            stat[pl.ds(base, CONV_ROWS), :] = jnp.where(
+                lane == 0, first_sum, jnp.where(lane == 1, square_sum, jnp.float32(0.0)))
+
+        stat_out[layer] = jnp.transpose(stat[...])[:8]
+        stat_copies = [
+            to_tp(stat_out.at[layer], stat_in.at[layer, t], ssend.at[layer, k], srecv.at[layer, t], (t + k) % m)
+            for k in range(1, m)]
+        for copy in stat_copies:
+            copy.start()
+        tend()
+        summed = stat_out[layer]
+        for k in range(1, m):
+            peer = (t + k) % m
+            to_tp(stat_in.at[layer, peer], stat_in.at[layer, peer], ssend.at[layer, k],
+                  srecv.at[layer, peer], peer).wait_recv()
+            summed = summed + stat_in[layer, peer]
+        stat[...] = jnp.transpose(
+            jnp.concatenate([summed, jnp.zeros((120, rows), jnp.float32)], axis=0))
+
+        mine = pl.ds(pl.multiple_of(t * block, block), block)
+
+        @pl.loop(0, rows // CONV_ROWS)
+        def _(i):
+            span = pl.ds(pl.multiple_of(i * CONV_ROWS, CONV_ROWS), CONV_ROWS)
+            both = stat[span, :]
+            row_mean = both[:, 0:1] / channels
+            row_var = both[:, 1:2] / channels - row_mean * row_mean
+            normalized = (ng_ref[pl.ds(layer, 1), :] * (conv[span, :] - row_mean)
+                          * lax.rsqrt(row_var + epsilon) + ns_ref[pl.ds(layer, 1), :])
+            act_all[layer, span, mine] = jax.nn.silu(normalized).astype(jnp.bfloat16)
+
+        def act_cols(who):
+            return act_all.at[layer, :, pl.ds(pl.multiple_of(who * block, block), block)]
+
+        partner = 2 * q + 1 - c
+        copies = []
+        for k in range(pairs - 1, -1, -1):
+            target_t = 2 * ((q + k) % pairs) + c if k else partner
+            copies.append(to_tp(act_cols(t), act_cols(t), asend.at[layer, k], arecv.at[layer, t], target_t))
+            copies[-1].start()
+        tend()
+        for k in range(1, pairs):
+            sender = 2 * ((q + k) % pairs) + c
+            to_tp(act_cols(sender), act_cols(sender), asend.at[layer, k], arecv.at[layer, sender], sender).wait_recv()
+            copies.append(to_tp(act_cols(sender), act_cols(sender), asend.at[layer, pairs + k],
+                                arecv.at[layer, sender], partner))
+            copies[-1].start()
+        tend()
+        ofull[layer, pl.ds(pl.multiple_of(t * block, block), block), :] = oring[
+            layer, :, pl.ds(pl.multiple_of(c * half_width, half_width), half_width)]
+        for k in range(1, m):
+            peer = (t + k) % m
+
+            @pl.loop(0, n)
+            def _(piece, peer=peer):
+                dst = ofull.at[layer, pl.ds(pl.multiple_of(peer * block, block), block),
+                               pl.ds(pl.multiple_of(piece * ho, ho), ho)]
+                to_tp(dst, dst, osend.at[layer, 0, 0, 0], orecv.at[layer, peer, piece], peer).wait_recv()
+
+        for k in range(pairs):
+            sender = 2 * ((q + k) % pairs) + 1 - c
+            to_tp(act_cols(sender), act_cols(sender), asend.at[layer, k], arecv.at[layer, sender], partner).wait_recv()
+        half = pl.ds(pl.multiple_of(c * half_width, half_width), half_width)
+        branch = jnp.dot(act_all[layer], ofull[layer], preferred_element_type=jnp.float32).astype(jnp.bfloat16)
+        target[:, half] = (source[:, half].astype(jnp.float32) + branch.astype(jnp.float32)).astype(jnp.bfloat16)
+        swap = to_tp(target.at[:, half], target.at[:, half], xsend.at[layer], xrecv.at[layer], partner)
+        swap.start()
+        tend()
+        swap.wait_recv()
+        tend()
+        if nxt is not None:
+            norm_rows(nxt, target)
+        tend()
+        for copy in copies + stat_copies + [halo_copy]:
+            copy.wait_send()
+        swap.wait_send()
+
+    for layer in range(layers):
+        layer_step(layer, tok_ref if layer == 0 else hid.at[layer - 1], hid.at[layer])
+    out_ref[...] = hid[layers - 1]
+
+    doc_copy.wait_send()
+
+    @pl.loop(0, n - 1)
+    def _(step):
+        for layer in range(layers):
+            for msg in range(3):
+                for way in range(2):
+                    ring_copy(layer, msg, way, step).wait_send()
+
+    @pl.loop(0, n)
+    def _(step):
+        for layer in range(layers):
+            for way in range(2):
+                spread(layer, way, step, "wait_send")
+
+
+def fused_on_device(n, m, tokens, doc_ids, pre_gain, value_proj, gate_proj, out_proj, conv_taps, norm_gain, norm_shift):
+    rows, width = tokens.shape
+    layers, depth, block = value_proj.shape
+    owidth = out_proj.shape[2]
+    reach = conv_taps.shape[1] - 1
+    channels = block * m
+    docs = jnp.broadcast_to(doc_ids[:, None], (rows, 128))
+    bf16, f32, i32 = jnp.bfloat16, jnp.float32, jnp.int32
+    dma = pltpu.SemaphoreType.DMA
+    vmem = pl.BlockSpec(memory_space=pltpu.VMEM)
+    return pl.pallas_call(
+        functools.partial(fused_kernel, n, m, reach, layers),
+        out_shape=jax.ShapeDtypeStruct((rows, width), bf16),
+        in_specs=[vmem] * 9,
+        out_specs=vmem,
+        scratch_shapes=[
+            pltpu.VMEM((layers, n * depth, 2 * block), bf16),
+            pltpu.VMEM((layers, block, n * owidth), bf16),
+            pltpu.VMEM((layers, channels, width // 2), bf16),
+            pltpu.VMEM((rows, width), bf16),
+            pltpu.VMEM((rows, 2 * block), f32),
+            pltpu.VMEM((block // 128 * (rows + HALO), 128), f32),
+            pltpu.VMEM((rows + HALO, 128), i32),
+            pltpu.VMEM((rows, 128), i32),
+            pltpu.VMEM((layers, HALO, block), bf16),
+            pltpu.VMEM((layers, HALO, block), bf16),
+            pltpu.VMEM((HALO, 128), i32),
+            pltpu.VMEM((rows, 128), f32),
+            pltpu.VMEM((layers, 8, rows), f32),
+            pltpu.VMEM((layers, m, 8, rows), f32),
+            pltpu.VMEM((rows, block), f32),
+            pltpu.VMEM((layers, rows, channels), bf16),
+            pltpu.VMEM((layers, rows, width), bf16),
+            dma((layers, 3, 2, n)), dma((layers, 3, 2, n)),
+            dma((layers, 2, n, m // 2)), dma((layers, m, n)),
+            dma((layers + 1,)), dma((layers + 1,)),
+            dma((layers, m)), dma((layers, m)),
+            dma((layers, m)), dma((layers, m)),
+            dma((layers,)), dma((layers,)),
+        ],
+        compiler_params=pltpu.CompilerParams(
+            collective_id=0, has_side_effects=True, vmem_limit_bytes=60 * 1024 * 1024),
+    )(tokens, docs, pre_gain, value_proj, gate_proj, out_proj, conv_taps, norm_gain, norm_shift)
 
 
 def passed_along(value, axis, steps):
@@ -69,9 +426,27 @@
     return hidden
 
 
+def suits_kernel(n, m, tokens, value_proj, out_proj, conv_taps):
+    rows, width = tokens.shape
+    depth, block = value_proj.shape[1:]
+    return (
+        n % 2 == 0 and 4 <= n <= 16 and m % 2 == 0 and m >= 4 and rows % 128 == 0 and width % 256 == 0
+        and depth % 32 == 0 and block % 128 == 0 and out_proj.shape[2] % 256 == 0
+        and conv_taps.shape[1] - 1 <= HALO
+    )
+
+
 def solution(mesh):
+    n, m = mesh.shape["sp"], mesh.shape["tp"]
+
+    def body(tokens, doc_ids, pre_gain, value_proj, gate_proj, out_proj, conv_taps, norm_gain, norm_shift):
+        chosen = on_device
+        if suits_kernel(n, m, tokens, value_proj, out_proj, conv_taps):
+            chosen = functools.partial(fused_on_device, n, m)
+        return chosen(tokens, doc_ids, pre_gain, value_proj, gate_proj, out_proj, conv_taps, norm_gain, norm_shift)
+
     return jax.shard_map(
-        on_device,
+        body,
         mesh=mesh,
         in_specs=(
             P("sp", None),

time: 282 us -> 104 us (0.37)
  waiting for transfers between devices: 218 us -> 0 us
  Pallas kernels: 0 us -> 98.2 us
  other arithmetic: 14.3 us -> 0 us
  between operations: 13.4 us -> 0.01 us
  blocking collectives: 12 us -> 0 us
  matrix products: 11.1 us -> 0 us
  starting transfers between devices: 10.9 us -> 0 us
  local copies, waits for them, and re-layouts: 1.85 us -> 5.66 us
    all_gather x3 -> x0, waiting for transfers between devices: 129 us -> none  [the longest x1 48 us: on_device(): lax.all_gather(gate_proj, 'sp', axis=1, tiled=True)]
    pallas_call x0 -> x1, Pallas kernels: none -> 98.2 us  [fused_on_device(): pl.pallas_call(functools.partial(fused_kernel, n, m, reach, layers), out_...]
    psum x2 -> x0, waiting for transfers between devices: 85 us -> none  [on_device(): summed = lax.psum(partial_value.astype(jnp.bfloat16), 'tp')]
    psum x2 -> x0, blocking collectives: 12 us -> none  [on_device(): lax.psum((jnp.sum(conv_out, axis=1), jnp.sum(conv_out * conv_out, axis=1)...]
    dot_general x6 -> x0, matrix products: 11.1 us -> none  [the longest x2 6.08 us: on_device(): jnp.dot(activated, full_out[layer_index], preferred_element_type=jnp.floa...]
    reduce_sum x4 -> x0, other arithmetic: 10.7 us -> none  [the longest x2 6.66 us: on_device(): jnp.sum(conv_out, axis=1)]
    ppermute x3 -> x0, starting transfers between devices: 10.7 us -> none  [passed_along(): lax.ppermute(value, axis, [(source, source + steps) for source in range(f...]
    convert_element_type x3 -> x0, other arithmetic: 3.24 us -> none  [the longest x1 3.16 us: on_device(): (hidden.astype(jnp.float32) + summed.astype(jnp.float32)).astype(jnp.bflo...]
  transfers between devices with their start and end apart: 8 -> 0, of which waited for: 7 -> 0; matrix products, arithmetic and copies ran while one was open for 4% -> 0% of each run, Pallas kernels for 0% -> 0%
where the time goes in v1:
time: 104 us
  Pallas kernels  98.2 us (94%)
  local copies, waits for them, and re-layouts  5.66 us (5%)
    pallas_call x1, Pallas kernels, fused_on_device(): pl.pallas_call(functools.partial(fused_kernel, n, m, reach, layers), out_...  98.2 us
    unnamed x2, local copies, waits for them, and re-layouts  4.18 us

profile of v1, /device:TPU:0, one launch (start us, length us, event | category | flops | bytes accessed | tf_op | source)
XLA Modules:
  0.0 103.9 jit_solution(9378029374809344037)
XLA Ops:
  0.0 1.5 %copy.10.tap_ref = f32[2,31,256]{2,1,0:T(8,128)} copy(f32[2,31,256]{2,0,1:T(2,128)} %param.15) | data formatting | bytes 126976 | tf_op args[6]
  1.5 1.5 %broadcast_in_dim.2.doc_ref = s32[384,128]{1,0:T(8,128)} broadcast(s32[384]{0:T(512)} %param.10), dimensions={0} | broadcast | bytes 198144 | tf_op jit(solution)/shard_map/broadcast_in_dim | solution.py:327
  2.9 98.2 %shard_map.91 = bf16[384,2048]{1,0:T(8,128)(2,1)} custom-call(bf16[384,2048]{1,0:T(8,128)(2,1)} %tok_ref.1, s32[384,128]{1,0:T(8,128)} %broadcast_in_dim.2.doc_ref, f32[2,2048]{1,0:T(2,128)} %gain_ref.1, bf16[2,256,256]{2,1,0:T(8,128)(2,1)} %v_ref.1, bf16[2,256,256]{2,1,0:T(8,128)(2,1)} %g_ref.1, bf16[2,256,256]{2,1,0:T(8,128)(2,1)} %o_ref.1, ...), custom_call_target="tpu_custom_call" | custom-call | tf_op jit(solution)/shard_map/pallas_call | solution.py:331
  101.2 2.7 %copy.12 = bf16[384,2048]{1,0:T(8,128)(2,1)} copy(bf16[384,2048]{1,0:T(8,128)(2,1)} %shard_map.91) | data formatting | bytes 3145728

commit v2 on v1

--- a/solution.py
+++ b/solution.py
@@ -16,7 +16,7 @@
     n, m, reach, layers,
     tok_ref, doc_ref, gain_ref, v_ref, g_ref, o_ref, tap_ref, ng_ref, ns_ref,
     out_ref,
-    w, oring, ofull, normed, acc, padded, pdoc, run, ghalo, halo_in, doc_in,
+    w, oring, ofull, normed, acc, padded, pdoc, run, ghalo, halo_in, doc_in, doc_tail,
     stat, stat_out, stat_in, conv, act_all, hid,
     rsend, rrecv, osend, orecv, hsend, hrecv, ssend, srecv, asend, arecv, xsend, xrecv,
 ):
@@ -100,12 +100,27 @@
             else:
                 getattr(copy, act)()
 
-    def open_ring(layer):
-        for msg in range(3):
-            for way in range(2):
-                ring_copy(layer, msg, way, 0, own=True).start()
+    def stream(layer, step, msgs):
         for way in range(2):
-            spread(layer, way, 0, "start", own=True)
+            if step > 0:
+                for msg in msgs:
+                    arrival(layer, msg, way, step - 1).wait_recv()
+                    if step < n - 1:
+                        ring_copy(layer, msg, way, step).start()
+            else:
+                for msg in msgs:
+                    ring_copy(layer, msg, way, 0, own=True).start()
+            if 2 in msgs:
+                spread(layer, way, step, "start", own=step == 0)
+
+    lag = min(3, n - 1)
+
+    def slot(time):
+        for layer in range(layers):
+            for msgs, late in (((0, 1), 0), ((2,), lag)):
+                step = time - (n - 1) * layer - late
+                if 0 <= step <= n - 1:
+                    stream(layer, step, msgs)
 
     def keep_own(layer):
         row = pl.ds(pl.multiple_of(me * depth, depth), depth)
@@ -113,27 +128,19 @@
         w[layer, row, pl.ds(block, block)] = g_ref[layer]
         oring[layer, :, pl.ds(pl.multiple_of(me * owidth, owidth), owidth)] = o_ref[layer]
 
-    def service(layer, first, last):
-        @pl.loop(first, last)
-        def _(step):
-            for msg in range(3):
-                for way in range(2):
-                    arrival(layer, msg, way, step - 1).wait_recv()
-                    ring_copy(layer, msg, way, step).start()
-            for way in range(2):
-                spread(layer, way, step, "start")
-
-    def finish_ring(layer):
-        for msg in range(3):
-            for way in range(2):
-                arrival(layer, msg, way, n - 2).wait_recv()
-        for way in range(2):
-            spread(layer, way, n - 1, "start")
-
-    open_ring(0)
-    doc_copy = to_sp(doc_ref.at[pl.ds(rows - HALO, HALO), :], doc_in, hsend.at[layers],
+    slot(0)
+
+    def doc_block(i):
+        row = doc_ref[pl.ds(i, 1), :].astype(jnp.float32)
+        return jnp.transpose(jnp.broadcast_to(row, (128, 128)))
+
+    doc_tail[...] = doc_block(rows // 128 - 1)[128 - HALO:]
+    doc_copy = to_sp(doc_tail, doc_in, hsend.at[layers],
                      hrecv.at[layers], following)
     doc_copy.start()
+
+    for i in range(rows // 128):
+        pdoc[pl.ds(HALO + i * 128, 128), :] = doc_block(i)
 
     def norm_rows(layer, source):
         @pl.loop(0, rows // 32)
@@ -145,40 +152,36 @@
 
     norm_rows(0, tok_ref)
     keep_own(0)
-    service(0, 1, 2)
+    slot(1)
     doc_copy.wait_recv()
-    pdoc[pl.ds(0, HALO), :] = jnp.where(me == 0, -1, doc_in[...])
-    pdoc[pl.ds(HALO, rows), :] = doc_ref[...]
+    pdoc[pl.ds(0, HALO), :] = jnp.where(me == 0, jnp.float32(-1.0), doc_in[...])
 
     @pl.loop(0, rows // CONV_ROWS)
     def _(i):
         base = pl.multiple_of(i * CONV_ROWS, CONV_ROWS)
         mine = pdoc[pl.ds(base + HALO, CONV_ROWS), :]
-        count = jnp.zeros_like(mine)
+        count = jnp.zeros((CONV_ROWS, 128), jnp.int32)
         for j in range(1, reach + 1):
             count = count + (pdoc[pl.ds(base + (HALO - j), CONV_ROWS), :] == mine).astype(jnp.int32)
         run[pl.ds(base, CONV_ROWS), :] = count
 
-    service(0, 2, n - 1)
-    if layers > 1:
-        for later in range(1, layers):
-            keep_own(later)
+    for later in range(1, layers):
+        keep_own(later)
+    for time in range(2, n):
+        slot(time)
 
     lane = lax.broadcasted_iota(jnp.int32, (CONV_ROWS, 128), 1)
 
     def layer_step(layer, source, target):
         nxt = layer + 1 if layer + 1 < layers else None
-        marks = iter([(1, 2), (2, 3), (3, 4), (4, 5), (5, 6), (6, n - 1)] if n == 8 else [(1, n - 1)])
+        opened = (n - 1) * (layer + 1) + 1
+        times = list(range(opened, opened + (n - 1 if nxt is not None else lag)))
+        shares = [times[i:i + 1] for i in range(6)] + [times[6:]]
 
         def tend():
-            if nxt is not None:
-                span = next(marks, None)
-                if span is not None:
-                    service(nxt, *span)
-
-        if nxt is not None:
-            open_ring(nxt)
-        finish_ring(layer)
+            for time in shares.pop(0):
+                slot(time)
+
         acc[...] = jnp.dot(normed[...], w[layer], preferred_element_type=jnp.float32)
 
         def store_padded(row, values):
@@ -214,9 +217,9 @@
             for part in range(block // 128):
                 cols = pl.ds(part * 128, 128)
                 lift = part * (rows + HALO)
-                total = tap_ref[layer, pl.ds(0, 1), cols] * padded[pl.ds(base + (lift + HALO), CONV_ROWS), :]
+                total = tap_ref[0, pl.ds(layer, 1), cols] * padded[pl.ds(base + (lift + HALO), CONV_ROWS), :]
                 for j in range(1, reach + 1):
-                    term = tap_ref[layer, pl.ds(j, 1), cols] * padded[pl.ds(base + (lift + HALO - j), CONV_ROWS), :]
+                    term = tap_ref[j, pl.ds(layer, 1), cols] * padded[pl.ds(base + (lift + HALO - j), CONV_ROWS), :]
                     total = total + jnp.where(count >= j, term, jnp.float32(0.0))
                 conv[pl.ds(base, CONV_ROWS), cols] = total
                 first_sum = first_sum + jnp.sum(total, axis=1, keepdims=True)
@@ -324,7 +327,7 @@
     owidth = out_proj.shape[2]
     reach = conv_taps.shape[1] - 1
     channels = block * m
-    docs = jnp.broadcast_to(doc_ids[:, None], (rows, 128))
+    docs = doc_ids.reshape(rows // 128, 128)
     bf16, f32, i32 = jnp.bfloat16, jnp.float32, jnp.int32
     dma = pltpu.SemaphoreType.DMA
     vmem = pl.BlockSpec(memory_space=pltpu.VMEM)
@@ -340,11 +343,12 @@
             pltpu.VMEM((rows, width), bf16),
             pltpu.VMEM((rows, 2 * block), f32),
             pltpu.VMEM((block // 128 * (rows + HALO), 128), f32),
-            pltpu.VMEM((rows + HALO, 128), i32),
+            pltpu.VMEM((rows + HALO, 128), f32),
             pltpu.VMEM((rows, 128), i32),
             pltpu.VMEM((layers, HALO, block), bf16),
             pltpu.VMEM((layers, HALO, block), bf16),
-            pltpu.VMEM((HALO, 128), i32),
+            pltpu.VMEM((HALO, 128), f32),
+            pltpu.VMEM((HALO, 128), f32),
             pltpu.VMEM((rows, 128), f32),
             pltpu.VMEM((layers, 8, rows), f32),
             pltpu.VMEM((layers, m, 8, rows), f32),
@@ -360,7 +364,7 @@
         ],
         compiler_params=pltpu.CompilerParams(
             collective_id=0, has_side_effects=True, vmem_limit_bytes=60 * 1024 * 1024),
-    )(tokens, docs, pre_gain, value_proj, gate_proj, out_proj, conv_taps, norm_gain, norm_shift)
+    )(tokens, docs, pre_gain, value_proj, gate_proj, out_proj, jnp.transpose(conv_taps, (1, 0, 2)), norm_gain, norm_shift)
 
 
 def passed_along(value, axis, steps):

time: 104 us -> 105 us (level)
  Pallas kernels: 98.2 us -> 102 us
  local copies, waits for them, and re-layouts: 5.66 us -> 2.73 us
    pallas_call x1, Pallas kernels: 98.2 us -> 102 us  [fused_on_device(): pl.pallas_call(functools.partial(fused_kernel, n, m, reach, layers), out_...]
    broadcast_in_dim x1 -> x0, local copies, waits for them, and re-layouts: 1.47 us -> none  [fused_on_device(): docs = jnp.broadcast_to(doc_ids[:, None], (rows, 128))]
    unnamed x2 -> x1, local copies, waits for them, and re-layouts: 4.18 us -> 2.73 us
where the time goes in v2:
time: 105 us
  Pallas kernels  102 us (97%)
  local copies, waits for them, and re-layouts  2.73 us (3%)
    pallas_call x1, Pallas kernels, fused_on_device(): pl.pallas_call(functools.partial(fused_kernel, n, m, reach, layers), out_...  102 us
    unnamed x1, local copies, waits for them, and re-layouts  2.73 us

profile of v2, /device:TPU:0, one launch (start us, length us, event | category | flops | bytes accessed | tf_op | source)
XLA Modules:
  0.0 104.7 jit_solution(10273821266209812069)
XLA Ops:
  0.0 102.0 %shard_map.91 = bf16[384,2048]{1,0:T(8,128)(2,1)} custom-call(bf16[384,2048]{1,0:T(8,128)(2,1)} %tok_ref.1, s32[3,128]{1,0:T(4,128)} %bitcast.3, f32[2,2048]{1,0:T(2,128)} %gain_ref.1, bf16[2,256,256]{2,1,0:T(8,128)(2,1)} %v_ref.1, bf16[2,256,256]{2,1,0:T(8,128)(2,1)} %g_ref.1, bf16[2,256,256]{2,1,0:T(8,128)(2,1)} %o_ref.1, f32[31,2,256]{2,1,0:T(2,128)} %bitcast.2, ...), custom_call_target="tpu_custom_call" | custom-call | tf_op jit(solution)/shard_map/pallas_call | solution.py:334
  102.0 2.7 %copy.11 = bf16[384,2048]{1,0:T(8,128)(2,1)} copy(bf16[384,2048]{1,0:T(8,128)(2,1)} %shard_map.91) | data formatting | bytes 3145728

commit v3 on v2

--- a/solution.py
+++ b/solution.py
@@ -100,27 +100,19 @@
             else:
                 getattr(copy, act)()
 
-    def stream(layer, step, msgs):
-        for way in range(2):
-            if step > 0:
-                for msg in msgs:
-                    arrival(layer, msg, way, step - 1).wait_recv()
+    def slot(time):
+        for layer in reversed(range(layers)):
+            step = time - (n - 1) * layer
+            if not 0 <= step <= n - 1:
+                continue
+            for msg in range(3):
+                for way in range(2):
+                    if step > 0:
+                        arrival(layer, msg, way, step - 1).wait_recv()
                     if step < n - 1:
-                        ring_copy(layer, msg, way, step).start()
-            else:
-                for msg in msgs:
-                    ring_copy(layer, msg, way, 0, own=True).start()
-            if 2 in msgs:
+                        ring_copy(layer, msg, way, step, own=step == 0).start()
+            for way in range(2):
                 spread(layer, way, step, "start", own=step == 0)
-
-    lag = min(3, n - 1)
-
-    def slot(time):
-        for layer in range(layers):
-            for msgs, late in (((0, 1), 0), ((2,), lag)):
-                step = time - (n - 1) * layer - late
-                if 0 <= step <= n - 1:
-                    stream(layer, step, msgs)
 
     def keep_own(layer):
         row = pl.ds(pl.multiple_of(me * depth, depth), depth)
@@ -175,7 +167,7 @@
     def layer_step(layer, source, target):
         nxt = layer + 1 if layer + 1 < layers else None
         opened = (n - 1) * (layer + 1) + 1
-        times = list(range(opened, opened + (n - 1 if nxt is not None else lag)))
+        times = list(range(opened, opened + n - 1)) if nxt is not None else []
         shares = [times[i:i + 1] for i in range(6)] + [times[6:]]
 
         def tend():
@@ -208,8 +200,7 @@
         halo_copy.wait_recv()
         store_padded(0, halo_in[layer])
 
-        @pl.loop(0, rows // CONV_ROWS)
-        def _(i):
+        def conv_rows(i):
             base = pl.multiple_of(i * CONV_ROWS, CONV_ROWS)
             count = run[pl.ds(base, CONV_ROWS), :]
             first_sum = jnp.zeros((CONV_ROWS, 1), jnp.float32)
@@ -227,6 +218,10 @@
             stat[pl.ds(base, CONV_ROWS), :] = jnp.where(
                 lane == 0, first_sum, jnp.where(lane == 1, square_sum, jnp.float32(0.0)))
 
+        middle = rows // CONV_ROWS // 2
+        pl.loop(0, middle)(conv_rows)
+        tend()
+        pl.loop(middle, rows // CONV_ROWS)(conv_rows)
         stat_out[layer] = jnp.transpose(stat[...])[:8]
         stat_copies = [
             to_tp(stat_out.at[layer], stat_in.at[layer, t], ssend.at[layer, k], srecv.at[layer, t], (t + k) % m)
@@ -293,7 +288,6 @@
         swap.start()
         tend()
         swap.wait_recv()
-        tend()
         if nxt is not None:
             norm_rows(nxt, target)
         tend()

time: 105 us -> 99.9 us (0.951)
  Pallas kernels: 102 us -> 97 us
    pallas_call x1, Pallas kernels: 102 us -> 97 us  [fused_on_device(): pl.pallas_call(functools.partial(fused_kernel, n, m, reach, layers), out_...]
where the time goes in v3:
time: 99.9 us; the launch traced here: 99.8 us
  Pallas kernels  97 us (97%)
  local copies, waits for them, and re-layouts  2.73 us (3%)
    pallas_call x1, Pallas kernels, fused_on_device(): pl.pallas_call(functools.partial(fused_kernel, n, m, reach, layers), out_...  97 us
    unnamed x1, local copies, waits for them, and re-layouts  2.73 us

profile of v3, /device:TPU:0, one launch (start us, length us, event | category | flops | bytes accessed | tf_op | source)
XLA Modules:
  0.0 99.8 jit_solution(14445615927979155627)
XLA Ops:
  0.0 97.0 %shard_map.91 = bf16[384,2048]{1,0:T(8,128)(2,1)} custom-call(bf16[384,2048]{1,0:T(8,128)(2,1)} %tok_ref.1, s32[3,128]{1,0:T(4,128)} %bitcast.3, f32[2,2048]{1,0:T(2,128)} %gain_ref.1, bf16[2,256,256]{2,1,0:T(8,128)(2,1)} %v_ref.1, bf16[2,256,256]{2,1,0:T(8,128)(2,1)} %g_ref.1, bf16[2,256,256]{2,1,0:T(8,128)(2,1)} %o_ref.1, f32[31,2,256]{2,1,0:T(2,128)} %bitcast.2, ...), custom_call_target="tpu_custom_call" | custom-call | tf_op jit(solution)/shard_map/pallas_call | solution.py:328
  97.1 2.7 %copy.11 = bf16[384,2048]{1,0:T(8,128)(2,1)} copy(bf16[384,2048]{1,0:T(8,128)(2,1)} %shard_map.91) | data formatting | bytes 3145728
